TPU v7x, 32 devices: a whole 2x2x4 slice. The times are simulated.
32 devices in a mesh: grp: 2 (over y), kv: 4 (over z), tp: 4 (over x, core).
Axes of the slice: x: 2, y: 2, z: 4, core: 2. Of those that a mesh axis runs over, the one named last changes fastest.
Arguments:
- tokens: bfloat16 [32, 4096], P('grp', 'kv'), parts along dimension 0, may hold values from -16 to 16
- positions: int32 [32], P(('grp', 'kv')), parts along dimension 0, may hold values from 512 to 8191
- state: float32 [32, 16, 128, 128], P(('grp', 'kv'), 'tp'), parts along dimension 0, may hold values from -3 to 3
- norm_gain: float32 [4096], P('kv'), may hold values from 0.1 to 1.9
- w_query: bfloat16 [4096, 2048], P('kv', 'tp'), may hold values from -0.09375 to 0.09375
- w_key: bfloat16 [4096, 2048], P('kv', 'tp'), may hold values from -0.09375 to 0.09375
- w_value: bfloat16 [4096, 2048], P('kv', 'tp'), may hold values from -0.09375 to 0.09375
- w_gate: bfloat16 [4096, 2048], P('kv', 'tp'), may hold values from -0.09375 to 0.09375
- w_out: bfloat16 [2048, 4096], P('tp', 'kv'), may hold values from -0.125 to 0.125
- mlp_gain: float32 [4096], P('kv'), may hold values from 0.1 to 1.9
- w_up: bfloat16 [4096, 16384], P('kv', 'tp'), may hold values from -0.09375 to 0.09375
- w_down: bfloat16 [16384, 4096], P('tp', 'kv'), may hold values from -0.046875 to 0.046875
Outputs:
- layer_out: bfloat16 [32, 4096], P('grp', 'kv'), parts along dimension 0
- new_state: float32 [32, 16, 128, 128], P(('grp', 'kv'), 'tp'), parts along dimension 0
There are 2 independent parts, one for each index of `grp`. A program takes and returns all parts, laid end to end along the dimension named above; an argument that names none is the same for every part. Nothing has to cross between parts.
All inputs are finite; a program needn't handle non-finite values.
Results may differ from a plain program's by a relative error of at most 0.007.
Values may be sent and summed in bfloat16 or wider, within the bound.
A program may use at most 64 MiB of HBM per device.

v0:
```python
import jax
import jax.numpy as jnp
from jax import lax
from jax.sharding import PartitionSpec as P

D = 4096
HEADS = 16


def turn(values, positions):
    half = values.shape[-1] // 2
    freq = 10000.0 ** (-(jnp.arange(half, dtype=jnp.float32) * 2.0) / values.shape[-1])
    angle = positions.astype(jnp.float32)[:, None, None] * freq[None, None, :]
    cosine = jnp.cos(angle)
    sine = jnp.sin(angle)
    first = values[..., :half]
    second = values[..., half:]
    return jnp.concatenate(
        [first * cosine - second * sine, first * sine + second * cosine], axis=-1
    )


def shards(
    tokens,
    positions,
    state,
    norm_gain,
    w_query,
    w_key,
    w_value,
    w_gate,
    w_out,
    mlp_gain,
    w_up,
    w_down,
):
    local_seqs, head_dev, head_size, _ = state.shape
    inputs = tokens.astype(jnp.float32)
    squares = jnp.sum(inputs * inputs, axis=1)
    normed = (inputs * norm_gain).astype(jnp.bfloat16)
    terms = jnp.stack(
        [
            jnp.dot(normed, weight, preferred_element_type=jnp.float32)
            for weight in (w_query, w_key, w_value, w_gate)
        ],
        axis=1,
    )
    summed, total_sq = (
        lax.psum_scatter(terms, "kv", scatter_dimension=0, tiled=True),
        lax.psum_scatter(squares, "kv", scatter_dimension=0, tiled=True),
    )
    scale1 = lax.rsqrt(total_sq / D + 1e-06)
    summed = (summed * scale1[:, None, None]).reshape(local_seqs, 4, head_dev, head_size)
    query = turn(summed[:, 0], positions)
    key_rows = turn(summed[:, 1], positions) * head_size ** (-0.5)
    value = summed[:, 2]
    gate = summed[:, 3]
    heads = (lax.axis_index("tp") * head_dev + jnp.arange(head_dev)).astype(jnp.float32)
    gamma = 1.0 - 2.0 ** (-5.0 - 5.0 * heads / (HEADS - 1))
    new_state = gamma[None, :, None, None] * state + key_rows[:, :, :, None] * value[:, :, None, :]
    read = jnp.einsum("bhd,bhde->bhe", query, new_state, precision=lax.Precision.HIGHEST)
    read = read * lax.rsqrt(jnp.mean(read * read, axis=-1, keepdims=True) + 1e-06)
    retained = (
        (read * jax.nn.silu(gate)).reshape(local_seqs, head_dev * head_size).astype(jnp.bfloat16)
    )
    head_terms = jnp.dot(
        lax.all_gather(retained, "kv", axis=0, tiled=True),
        w_out,
        preferred_element_type=jnp.float32,
    )
    mixed = (inputs + lax.psum(head_terms, "tp")).astype(jnp.bfloat16)
    middle = mixed.astype(jnp.float32)
    squares2 = jnp.sum(middle * middle, axis=1)
    normed2 = (middle * mlp_gain).astype(jnp.bfloat16)
    upward = jnp.dot(normed2, w_up, preferred_element_type=jnp.float32)
    up_full, total_sq2 = lax.psum((upward, squares2), "kv")
    scale2 = lax.rsqrt(total_sq2 / D + 1e-06)
    hidden = jnp.square(jax.nn.relu(up_full * scale2[:, None])).astype(jnp.bfloat16)
    down_terms = jnp.dot(hidden, w_down, preferred_element_type=jnp.float32)
    layer_out = (middle + lax.psum(down_terms, "tp")).astype(jnp.bfloat16)
    return (layer_out, new_state)


def solution(mesh):
    return jax.shard_map(
        shards,
        mesh=mesh,
        in_specs=(
            P("grp", "kv"),
            P(("grp", "kv")),
            P(("grp", "kv"), "tp", None, None),
            P("kv"),
            P("kv", "tp"),
            P("kv", "tp"),
            P("kv", "tp"),
            P("kv", "tp"),
            P("tp", "kv"),
            P("kv"),
            P("kv", "tp"),
            P("tp", "kv"),
        ),
        out_specs=(P("grp", "kv"), P(("grp", "kv"), "tp", None, None)),
        check_vma=False,
    )
```

profile of v0, /device:TPU:0, one launch (start us, length us, event | category | flops | bytes accessed | tf_op | source)
XLA Modules:
  0.0 187.9 jit_solution(12907306079230193447)
XLA Ops:
  7.2 0.0 copy-start
  7.2 0.0 copy-start.2
  7.2 0.0 copy-start.3
  7.2 0.0 all-reduce.13.cloned.1.call-start
  7.2 1.6 convolution_bitcast_fusion.3
  8.8 1.5 convolution_bitcast_fusion.2
  10.3 1.5 convolution_bitcast_fusion.1
  11.8 1.5 convolution_bitcast_fusion
  13.4 0.7 pad_maximum_fusion
  14.0 0.0 all-reduce.13.cloned.1.call-update
  14.1 0.0 all-reduce.7.cloned.1.call-start
  14.1 0.9 fusion.4
  15.0 0.7 convert_element_type.40
  15.7 0.1 multiply_cosine_fusion
  15.8 1.2 dynamic-slice
  17.7 13.5 %all-reduce.1 = f32[16]{0:T(128)S(1)} all-reduce(f32[16]{0:T(128)S(1)} %fusion.4), channel_id=3, replica_groups=mesh['grp'=2,'kv'=4,'tp'=4] {'kv'}, use_global_device_ids=true, to_apply=%region_2.0.clone | all-reduce | flops 16 | bytes 128
  31.2 0.1 fusion.19
  31.3 20.3 %all-reduce.13.cloned.1.call-done = f32[16,4,512]{2,0,1:T(8,128)} async-done(((f32[16,4,512]{2,0,1:T(8,128)}), f32[16,4,512]{2,0,1:T(8,128)}) %all-reduce.13.cloned.1.call-update) | async-done | bytes 131088
  51.6 0.9 dynamic-slice_multiply_fusion
  52.5 0.1 multiply_subtract_fusion
  52.6 0.1 pad_maximum_fusion.1
  52.7 1.6 multiply_add_fusion
  54.3 0.0 copy-start.1
  54.3 1.0 fusion.22
  55.3 0.1 multiply_reduce_fusion
  55.4 0.1 fusion.17
  55.5 13.2 %all-gather = bf16[4,4,512]{2,1,0:T(4,128)(2,1)S(1)} all-gather(bf16[1,4,512]{2,1,0:T(4,128)(2,1)S(1)} %reshape.108), channel_id=1, replica_groups=mesh['grp'=2,'kv'=4,'tp'=4] {'kv'}, dimensions={0}, use_global_device_ids=true | all-gather | bytes 20480 | tf_op jit(solution)/shard_map/all_gather | solution.py:67
  68.7 0.0 copy-done
  68.7 0.9 fusion.23
  69.6 0.0 all-reduce.7.cloned.1.call-update
  69.6 0.0 all-reduce.9.cloned.1.call-start
  69.6 31.3 %all-reduce.7.cloned.1.call-done = f32[16,1024]{1,0:T(8,128)} async-done(((f32[16,1024]{1,0:T(8,128)}), f32[16,1024]{1,0:T(8,128)}) %all-reduce.7.cloned.1.call-update) | async-done | bytes 65552 | tf_op jit(solution)/shard_map/psum | solution.py:71
  101.0 0.0 copy-done.2
  101.0 1.0 fusion.7
  101.9 0.0 copy-done.3
  101.9 5.3 %fusion.9 = f32[16,4096]{1,0:T(8,128)} fusion(bf16[1024,4096]{1,0:T(8,128)(2,1)} %param.22, bf16[16,1024]{1,0:T(8,128)(2,1)S(1)} %get-tuple-element.3, f32[1024]{0:T(1024)S(1)} %copy-done.3), kind=kOutput, calls=%fused_computation.22 | convolution fusion | flops 134266880 | bytes 8687616 | tf_op jit(solution)/shard_map/dot_general | solution.py:75
  107.2 0.0 copy-done.1
  107.2 0.0 all-reduce.9.cloned.1.call-update
  107.2 0.0 all-reduce.11.cloned.1.call-start
  107.3 11.8 %psum.30 = f32[16]{0:T(128)S(1)} all-reduce(f32[16]{0:T(128)S(1)} %get-tuple-element.2), channel_id=1, replica_groups=mesh['grp'=2,'kv'=4,'tp'=4] {'kv'}, use_global_device_ids=true, to_apply=%region_7.8 | all-reduce | flops 16 | bytes 128 | tf_op jit(solution)/shard_map/psum | solution.py:76
  119.1 23.9 %all-reduce.9.cloned.1.call-done = f32[16,4096]{1,0:T(8,128)} async-done(((f32[16,4096]{1,0:T(8,128)}), f32[16,4096]{1,0:T(8,128)}) %all-reduce.9.cloned.1.call-update) | async-done | bytes 262160 | tf_op jit(solution)/shard_map/psum | solution.py:76
  143.0 5.3 %fusion = f32[16,1024]{1,0:T(8,128)} fusion(bf16[4096,1024]{1,0:T(8,128)(2,1)} %param.23, f32[16,4096]{1,0:T(8,128)} %all-reduce.9.cloned.1.call-done, f32[16]{0:T(128)S(1)} %add_rsqrt_fusion.1), kind=kOutput, calls=%fused_computation.6 | convolution fusion | flops 134479872 | bytes 8716352 | tf_op jit(solution)/shard_map/dot_general | solution.py:79
  148.3 0.0 all-reduce.11.cloned.1.call-update
  148.4 31.6 %all-reduce.11.cloned.1.call-done = f32[16,1024]{1,0:T(8,128)} async-done(((f32[16,1024]{1,0:T(8,128)}), f32[16,1024]{1,0:T(8,128)}) %all-reduce.11.cloned.1.call-update) | async-done | bytes 65552 | tf_op jit(solution)/shard_map/psum | solution.py:80
  179.9 1.5 fusion.8
  (8 shorter events, 0.1 us)
Async XLA Ops:
  7.2 61.5 %copy-start = (bf16[512,1024]{1,0:T(8,128)(2,1)S(1)}, bf16[512,1024]{1,0:T(8,128)(2,1)}, u32[]{:S(2)}) copy-start(bf16[512,1024]{1,0:T(8,128)(2,1)} %param.20) | copy-start | bytes 3145732
  7.2 93.8 %copy-start.2 = (bf16[16,1024]{1,0:T(8,128)(2,1)S(1)}, bf16[16,1024]{1,0:T(8,128)(2,1)}, u32[]{:S(2)}) copy-start(bf16[16,1024]{1,0:T(8,128)(2,1)} %param.12) | copy-start | bytes 98308
  7.2 94.7 %copy-start.3 = (f32[1024]{0:T(1024)S(1)}, f32[1024]{0:T(1024)}, u32[]{:S(2)}) copy-start(f32[1024]{0:T(1024)} %param.21) | copy-start | bytes 12292
  7.2 44.4 %all-reduce.13.cloned.1.call-start = ((), (), s32[]{:S(2)}) async-start(), calls=%async_computation.3 | async-start | bytes 262144
  14.1 86.9 %all-reduce.7.cloned.1.call-start = ((), (), s32[]{:S(2)}) async-start(), calls=%async_computation | async-start | bytes 131072 | tf_op jit(solution)/shard_map/psum | solution.py:71
  54.3 52.9 %copy-start.1 = (f32[4,4,128,128]{3,2,1,0:T(8,128)}, f32[4,4,128,128]{3,2,1,0:T(8,128)S(1)}, u32[]{:S(2)}) copy-start(f32[4,4,128,128]{3,2,1,0:T(8,128)S(1)} %multiply_add_fusion) | copy-start | bytes 3145732
  69.6 73.4 %all-reduce.9.cloned.1.call-start = ((), (), s32[]{:S(2)}) async-start(), calls=%async_computation.1 | async-start | bytes 524288 | tf_op jit(solution)/shard_map/psum | solution.py:76
  107.2 72.7 %all-reduce.11.cloned.1.call-start = ((), (), s32[]{:S(2)}) async-start(), calls=%async_computation.2 | async-start | bytes 131072 | tf_op jit(solution)/shard_map/psum | solution.py:80
Sparse Core Ops, SparseCore 0:
  14.2 37.3 all-reduce.12
  69.7 31.1 all-reduce.6
  107.4 35.5 all-reduce.8
  148.5 31.3 all-reduce.10
where the time goes:
time: 189 us; the launch traced here: 188 us
  waiting for transfers between devices  107 us (57%)
  blocking collectives  38.5 us (20%)
  matrix products  18.6 us (10%)
  between operations  14.5 us (8%)
  other arithmetic  7.69 us (4%)
    psum x1, waiting for transfers between devices, shards(): layer_out = (middle + lax.psum(down_terms, 'tp')).astype(jnp.bfloat16)  31.6 us
    psum x1, waiting for transfers between devices, shards(): mixed = (inputs + lax.psum(head_terms, 'tp')).astype(jnp.bfloat16)  31.3 us
    psum x1, waiting for transfers between devices, shards(): up_full, total_sq2 = lax.psum((upward, squares2), 'kv')  23.9 us
    unnamed x5, waiting for transfers between devices  20.4 us
    unnamed x1, blocking collectives  13.5 us
    all_gather x1, blocking collectives, shards(): lax.all_gather(retained, 'kv', axis=0, tiled=True)  13.2 us
    psum x1, blocking collectives, shards(): up_full, total_sq2 = lax.psum((upward, squares2), 'kv')  11.8 us
    dot_general x4, matrix products, shards(): jnp.dot(normed, weight, preferred_element_type=jnp.float32)  6.11 us
  transfers between devices with their start and end apart: 4, of which 4 were waited for; matrix products, arithmetic and copies ran while one was open for 2% of the time, Pallas kernels for 0%

commit v1 on v0

v1 whole, which is shorter than its diff:
```python
import functools

import jax
import jax.numpy as jnp
import numpy as np
from jax import lax
from jax.experimental import pallas as pl
from jax.experimental.pallas import tpu as pltpu
from jax.sharding import PartitionSpec as P

D = 4096
HEADS = 16
MESH = pl.DeviceIdType.MESH
F32 = jnp.float32
BF16 = jnp.bfloat16


def tile_of(width):
    return 512 if width % 512 == 0 else (256 if width % 256 == 0 else 128)


def lane_fill(column):
    return jnp.broadcast_to(column, (column.shape[0], 128))


def split_high_low(column):
    high = column.astype(BF16)
    low = (column - high.astype(F32)).astype(BF16)
    return jnp.concatenate([lane_fill(high.astype(F32)), lane_fill(low.astype(F32))], axis=1)


def kernel(
    kv, tp, chunks,
    positions, tokens, state, norm_gain, freq, w_query, w_key, w_value, w_gate, w_out, mlp_gain, w_up, w_down,
    out_ref, new_state,
    tok_v, gain1_v, gain2_v, freq_v, wq_v, wk_v, wv_v, wg_v, wo_v, wu_v, wd_v, st_v,
    send1, recv1, ret, mix, send2, recv2, sums2, rsums2, hid, down, out_v,
    load_sem, s1_sem, r1_sem, sr_sem, rr_sem, sm_sem, rm_sem, s2_sem, r2_sem, ss_sem, rs_sem, sh_sem, rh_sem,
    sd_sem, rd_sem, store_sem,
):
    me_kv = lax.axis_index("kv")
    me_tp = lax.axis_index("tp")
    rows, width = tok_v.shape
    seqs = rows // kv
    ret_width = wq_v.shape[1]
    head_size = st_v.shape[-1]
    heads = st_v.shape[1]
    ff = wu_v.shape[1]
    cw = ff // chunks

    loads = []

    def load(src, dst):
        copy = pltpu.make_async_copy(src, dst, load_sem.at[len(loads)])
        loads.append(copy)
        copy.start()
        return copy

    l_tok = load(tokens, tok_v)
    l_g1 = load(norm_gain, gain1_v)
    l_w = [load(a, b) for a, b in ((w_query, wq_v), (w_key, wk_v), (w_value, wv_v), (w_gate, wg_v))]
    l_freq = load(freq, freq_v)
    l_state = load(state, st_v)
    l_wo = load(w_out, wo_v)
    l_g2 = load(mlp_gain, gain2_v)
    l_up = [load(w_up.at[:, pl.ds(c * cw, cw)], wu_v.at[:, pl.ds(c * cw, cw)]) for c in range(chunks)]
    l_down = [load(w_down.at[pl.ds(c * cw, cw), :], wd_v.at[pl.ds(c * cw, cw), :]) for c in range(chunks)]

    barrier = pltpu.get_barrier_semaphore()
    for s in range(1, kv):
        pl.semaphore_signal(barrier, inc=1, device_id={"kv": lax.rem(me_kv + s, kv)}, device_id_type=MESH)
    for s in range(1, tp):
        pl.semaphore_signal(barrier, inc=1, device_id={"tp": lax.rem(me_tp + s, tp)}, device_id_type=MESH)

    def remote(src, dst, send_sem, recv_sem, axis, target):
        copy = pltpu.make_async_remote_copy(
            src_ref=src, dst_ref=dst, send_sem=send_sem, recv_sem=recv_sem,
            device_id={axis: target}, device_id_type=MESH,
        )
        copy.start()
        return copy

    l_tok.wait()
    l_g1.wait()
    inputs = tok_v[...].astype(F32)
    normed = (inputs * gain1_v[...]).astype(BF16)
    extra = split_high_low(jnp.sum(inputs * inputs, axis=1, keepdims=True))
    for j in range(kv):
        send1[j, :, 4 * ret_width:] = extra[j * seqs:(j + 1) * seqs].astype(BF16)

    l_freq.wait()
    row = lax.broadcasted_iota(jnp.int32, (seqs, head_size), 0)
    lane = lax.broadcasted_iota(jnp.int32, (seqs, head_size), 1)
    pos = jnp.zeros((seqs, head_size), F32)
    for b in range(seqs):
        pos = jnp.where(row == b, positions[b].astype(F32), pos)
    angle = pos * freq_v[...]
    cosine = jnp.cos(angle)
    sine = jnp.where(lane < head_size // 2, -1.0, 1.0) * jnp.sin(angle)

    t1 = tile_of(ret_width)
    for i, weight in enumerate((wq_v, wk_v, wv_v, wg_v)):
        l_w[i].wait()
        for n in range(ret_width // t1):
            term = jnp.dot(normed, weight[:, n * t1:(n + 1) * t1], preferred_element_type=F32)
            at = i * ret_width + n * t1
            for j in range(kv):
                send1[j, :, at:at + t1] = term[j * seqs:(j + 1) * seqs].astype(BF16)

    pl.semaphore_wait(barrier, kv + tp - 2)
    pending = []
    copies = []
    for s in range(1, kv):
        to = lax.rem(me_kv + s, kv)
        copies.append(remote(send1.at[to], recv1.at[s - 1], s1_sem.at[s - 1], r1_sem.at[s - 1], "kv", to))
    pending += copies
    summed = send1[me_kv].astype(F32)
    for s in range(1, kv):
        copies[s - 1].wait_recv()
        summed = summed + recv1[s - 1].astype(F32)
    total = summed[:, 4 * ret_width:4 * ret_width + 1] + summed[:, 4 * ret_width + 128:4 * ret_width + 129]
    scale1 = lax.rsqrt(total / D + 1e-06)

    def stack(i):
        base = i * ret_width
        return jnp.concatenate(
            [summed[:, base + h * head_size:base + (h + 1) * head_size] * scale1 for h in range(heads)], axis=0
        )

    cos_all = jnp.concatenate([cosine] * heads, axis=0)
    sin_all = jnp.concatenate([sine] * heads, axis=0)

    def turn(x):
        return x * cos_all + pltpu.roll(x, head_size // 2, 1) * sin_all

    count = seqs * heads
    query = turn(stack(0))
    key = turn(stack(1)) * head_size ** (-0.5)
    value = stack(2)
    gate = stack(3)
    columns = jnp.transpose(
        jnp.concatenate([query, key, jnp.zeros((128 - 2 * count, head_size), F32)], axis=0)
    )
    l_state.wait()
    reads = []
    for h in range(heads):
        index = (me_tp * heads + h).astype(F32)
        gamma = 1.0 - jnp.exp2(jnp.full((1, head_size), -5.0, F32) - 5.0 * index / (HEADS - 1))
        for b in range(seqs):
            at = h * seqs + b
            fresh = gamma * st_v[b, h] + columns[:, count + at:count + at + 1] * value[at:at + 1, :]
            st_v[b, h] = fresh
            reads.append(jnp.sum(columns[:, at:at + 1] * fresh, axis=0, keepdims=True))
    read = jnp.concatenate(reads, axis=0)
    read = read * lax.rsqrt(jnp.mean(read * read, axis=-1, keepdims=True) + 1e-06)
    kept = read * (gate / (1.0 + jnp.exp(-gate)))
    for h in range(heads):
        ret[me_kv, :, h * head_size:(h + 1) * head_size] = kept[h * seqs:(h + 1) * seqs].astype(BF16)
    copies = []
    for s in range(1, kv):
        to = lax.rem(me_kv + s, kv)
        copies.append(remote(ret.at[me_kv], ret.at[me_kv], sr_sem.at[s - 1], rr_sem.at[s - 1], "kv", to))
    pending += copies
    store_state = pltpu.make_async_copy(st_v, new_state, store_sem.at[0])
    store_state.start()
    l_wo.wait()
    for s in range(1, kv):
        copies[s - 1].wait_recv()
    retained = jnp.concatenate([ret[j].astype(F32) for j in range(kv)], axis=0).astype(BF16)

    def reduce_tp(terms_into, buffer, send_sem, recv_sem):
        terms_into()
        sent = []
        for s in range(1, tp):
            to = lax.rem(me_tp + s, tp)
            sent.append(remote(buffer.at[me_tp], buffer.at[me_tp], send_sem.at[s - 1], recv_sem.at[s - 1], "tp", to))
        for s in range(1, tp):
            sent[s - 1].wait_recv()
        result = buffer[0].astype(F32)
        for j in range(1, tp):
            result = result + buffer[j].astype(F32)
        return result, sent

    t2 = tile_of(width)

    def out_terms():
        for n in range(width // t2):
            cols = slice(n * t2, (n + 1) * t2)
            mix[me_tp, :, cols] = jnp.dot(retained, wo_v[:, cols], preferred_element_type=F32).astype(BF16)

    head_sum, sent = reduce_tp(out_terms, mix, sm_sem, rm_sem)
    pending += sent
    mixed = (inputs + head_sum).astype(BF16)
    middle = mixed.astype(F32)
    l_g2.wait()
    normed2 = (middle * gain2_v[...]).astype(BF16)
    extra = split_high_low(jnp.sum(middle * middle, axis=1, keepdims=True))
    for j in range(kv):
        sums2[j] = extra[j * seqs:(j + 1) * seqs].astype(BF16)
    sum_copies = []
    for s in range(1, kv):
        to = lax.rem(me_kv + s, kv)
        sum_copies.append(remote(sums2.at[to], rsums2.at[s - 1], ss_sem.at[s - 1], rs_sem.at[s - 1], "kv", to))
    pending += sum_copies

    t3 = tile_of(cw)
    up_copies = []
    for c in range(chunks):
        l_up[c].wait()

        @pl.loop(0, cw // t3)
        def _(n, c=c):
            start = pl.multiple_of(n * t3, t3)
            term = jnp.dot(normed2, wu_v[:, pl.ds(c * cw + start, t3)], preferred_element_type=F32)
            for j in range(kv):
                send2[c, j, :, pl.ds(start, t3)] = term[j * seqs:(j + 1) * seqs].astype(BF16)

        row_copies = []
        for s in range(1, kv):
            to = lax.rem(me_kv + s, kv)
            row_copies.append(
                remote(send2.at[c, to], recv2.at[c, s - 1], s2_sem.at[c, s - 1], r2_sem.at[c, s - 1], "kv", to)
            )
        up_copies.append(row_copies)
        pending += row_copies

    sums = sums2[me_kv].astype(F32)
    for s in range(1, kv):
        sum_copies[s - 1].wait_recv()
        sums = sums + rsums2[s - 1].astype(F32)
    scale2 = lax.rsqrt((sums[:, :1] + sums[:, 128:129]) / D + 1e-06)

    hid_copies = []
    for c in range(chunks):
        up_sum = send2[c, me_kv].astype(F32)
        for s in range(1, kv):
            up_copies[c][s - 1].wait_recv()
            up_sum = up_sum + recv2[c, s - 1].astype(F32)
        positive = jnp.maximum(up_sum * scale2, 0.0)
        hid[c, me_kv] = (positive * positive).astype(BF16)
        row_copies = []
        for s in range(1, kv):
            to = lax.rem(me_kv + s, kv)
            row_copies.append(
                remote(hid.at[c, me_kv], hid.at[c, me_kv], sh_sem.at[c, s - 1], rh_sem.at[c, s - 1], "kv", to)
            )
        hid_copies.append(row_copies)
        pending += row_copies

    for c in range(chunks):
        l_down[c].wait()
        for s in range(1, kv):
            hid_copies[c][s - 1].wait_recv()
        hidden = jnp.concatenate([hid[c, j].astype(F32) for j in range(kv)], axis=0).astype(BF16)

        @pl.loop(0, width // t2)
        def _(n, c=c, hidden=hidden):
            cols = pl.ds(pl.multiple_of(n * t2, t2), t2)
            term = jnp.dot(hidden, wd_v[pl.ds(c * cw, cw), cols], preferred_element_type=F32)
            if c == 0:
                out_v[:, cols] = term
            else:
                out_v[:, cols] += term

    def down_terms():
        down[me_tp] = out_v[...].astype(BF16)

    down_sum, sent = reduce_tp(down_terms, down, sd_sem, rd_sem)
    pending += sent
    out_ref[...] = (middle + down_sum).astype(BF16)
    for copy in pending:
        copy.wait_send()
    store_state.wait()


def solution(mesh):
    kv, tp = mesh.shape["kv"], mesh.shape["tp"]

    def shards(
        tokens, positions, state, norm_gain, w_query, w_key, w_value, w_gate, w_out, mlp_gain, w_up, w_down
    ):
        rows, width = tokens.shape
        seqs, heads, head_size, _ = state.shape
        ret_width = w_query.shape[1]
        ff = w_up.shape[1]
        chunks = 4
        cw = ff // chunks
        half = head_size // 2
        table = 10000.0 ** (-(np.arange(half) * 2.0) / head_size)
        freq = jnp.asarray(np.concatenate([table, table])[None, :], F32)
        any_spec = pl.BlockSpec(memory_space=pl.ANY)
        vmem = pltpu.VMEM
        dma = pltpu.SemaphoreType.DMA
        block1 = 4 * ret_width + 256
        return pl.pallas_call(
            functools.partial(kernel, kv, tp, chunks),
            name="layer",
            out_shape=(
                jax.ShapeDtypeStruct((rows, width), BF16),
                jax.ShapeDtypeStruct(state.shape, F32),
            ),
            in_specs=[pl.BlockSpec(memory_space=pltpu.SMEM)] + [any_spec] * 12,
            out_specs=(pl.BlockSpec(memory_space=pltpu.VMEM), any_spec),
            scratch_shapes=[
                vmem((rows, width), BF16),
                vmem((1, width), F32),
                vmem((1, width), F32),
                vmem((1, head_size), F32),
                vmem(w_query.shape, BF16),
                vmem(w_key.shape, BF16),
                vmem(w_value.shape, BF16),
                vmem(w_gate.shape, BF16),
                vmem(w_out.shape, BF16),
                vmem(w_up.shape, BF16),
                vmem(w_down.shape, BF16),
                vmem(state.shape, F32),
                vmem((kv, seqs, block1), BF16),
                vmem((kv - 1, seqs, block1), BF16),
                vmem((kv, seqs, ret_width), BF16),
                vmem((tp, rows, width), BF16),
                vmem((chunks, kv, seqs, cw), BF16),
                vmem((chunks, kv - 1, seqs, cw), BF16),
                vmem((kv, seqs, 256), BF16),
                vmem((kv - 1, seqs, 256), BF16),
                vmem((chunks, kv, seqs, cw), BF16),
                vmem((tp, rows, width), BF16),
                vmem((rows, width), F32),
                dma((10 + 2 * chunks,)),
                dma((kv - 1,)), dma((kv - 1,)),
                dma((kv - 1,)), dma((kv - 1,)),
                dma((tp - 1,)), dma((tp - 1,)),
                dma((chunks, kv - 1)), dma((chunks, kv - 1)),
                dma((kv - 1,)), dma((kv - 1,)),
                dma((chunks, kv - 1)), dma((chunks, kv - 1)),
                dma((tp - 1,)), dma((tp - 1,)),
                dma((1,)),
            ],
            compiler_params=pltpu.CompilerParams(
                collective_id=0, has_side_effects=True, vmem_limit_bytes=60 * 1024 * 1024
            ),
        )(
            positions, tokens, state, norm_gain[None, :], freq, w_query, w_key, w_value, w_gate, w_out,
            mlp_gain[None, :], w_up, w_down,
        )

    return jax.shard_map(
        shards,
        mesh=mesh,
        in_specs=(
            P("grp", "kv"),
            P(("grp", "kv")),
            P(("grp", "kv"), "tp", None, None),
            P("kv"),
            P("kv", "tp"),
            P("kv", "tp"),
            P("kv", "tp"),
            P("kv", "tp"),
            P("tp", "kv"),
            P("kv"),
            P("kv", "tp"),
            P("tp", "kv"),
        ),
        out_specs=(P("grp", "kv"), P(("grp", "kv"), "tp", None, None)),
        check_vma=False,
    )
```

time: 189 us -> 36.9 us (0.20)
  waiting for transfers between devices: 107 us -> 0 us
  blocking collectives: 38.5 us -> 0 us
  Pallas kernels: 0 us -> 32.4 us
  matrix products: 18.6 us -> 0 us
  between operations: 14.5 us -> 0.64 us
  other arithmetic: 7.69 us -> 0 us
  local copies, waits for them, and re-layouts: 1.33 us -> 3.67 us
    psum x3 -> x0, waiting for transfers between devices: 86.8 us -> none  [the longest x1 31.6 us: shards(): layer_out = (middle + lax.psum(down_terms, 'tp')).astype(jnp.bfloat16)]
    pallas_call x0 -> x1, Pallas kernels: none -> 32.4 us  [shards(): pl.pallas_call(functools.partial(kernel, kv, tp, chunks), name='layer', o...]
    unnamed x5 -> x0, waiting for transfers between devices: 20.4 us -> none
    dot_general x8 -> x0, matrix products: 18.6 us -> none  [the longest x4 6.11 us: shards(): jnp.dot(normed, weight, preferred_element_type=jnp.float32)]
    unnamed x1 -> x0, blocking collectives: 13.5 us -> none
    all_gather x1 -> x0, blocking collectives: 13.2 us -> none  [shards(): lax.all_gather(retained, 'kv', axis=0, tiled=True)]
    psum x1 -> x0, blocking collectives: 11.8 us -> none  [shards(): up_full, total_sq2 = lax.psum((upward, squares2), 'kv')]
    unnamed x11 -> x2, local copies, waits for them, and re-layouts: 1.3 us -> 3.67 us
  transfers between devices with their start and end apart: 4 -> 0, of which waited for: 4 -> 0; matrix products, arithmetic and copies ran while one was open for 2% -> 0% of each run, Pallas kernels for 0% -> 0%
where the time goes in v1:
time: 36.9 us; the launch traced here: 36.7 us
  Pallas kernels  32.4 us (88%)
  local copies, waits for them, and re-layouts  3.67 us (10%)
  between operations  0.64 us (2%)
    pallas_call x1, Pallas kernels, shards(): pl.pallas_call(functools.partial(kernel, kv, tp, chunks), name='layer', o...  32.4 us
    unnamed x2, local copies, waits for them, and re-layouts  3.67 us

profile of v1, /device:TPU:0, one launch (start us, length us, event | category | flops | bytes accessed | tf_op | source)
XLA Modules:
  0.0 36.7 jit_solution(2818711864478277974)
XLA Ops:
  0.6 32.4 %layer.1 = (bf16[16,1024]{1,0:T(8,128)(2,1)}, f32[4,4,128,128]{3,2,1,0:T(8,128)}) custom-call(s32[4]{0:T(128)} %positions.1, bf16[16,1024]{1,0:T(8,128)(2,1)} %tokens.1, f32[4,4,128,128]{3,2,1,0:T(8,128)} %state.1, f32[1,1024]{1,0:T(1,128)} %bitcast.2, f32[1,128]{1,0:T(1,128)} %constant.2.clone.freq, bf16[1024,512]{1,0:T(8,128)(2,1)} %w_query.1, ...), custom_call_target="tpu_custom_call" | custom-call | tf_op jit(solution)/shard_map/layer/pallas_call | solution.py:295
  33.0 1.4 %copy.17 = bf16[16,1024]{1,0:T(8,128)(2,1)} copy(bf16[16,1024]{1,0:T(8,128)(2,1)} %get-tuple-element.4) | data formatting | bytes 65536
  34.4 2.3 %copy.18 = f32[4,4,128,128]{3,2,1,0:T(8,128)} copy(f32[4,4,128,128]{3,2,1,0:T(8,128)} %get-tuple-element.5) | data formatting | bytes 2097152

commit v2 on v1

--- a/solution.py
+++ b/solution.py
@@ -32,11 +32,11 @@
 def kernel(
     kv, tp, chunks,
     positions, tokens, state, norm_gain, freq, w_query, w_key, w_value, w_gate, w_out, mlp_gain, w_up, w_down,
-    out_ref, new_state,
-    tok_v, gain1_v, gain2_v, freq_v, wq_v, wk_v, wv_v, wg_v, wo_v, wu_v, wd_v, st_v,
+    out_ref, st_v,
+    pos_s, tok_v, gain1_v, gain2_v, freq_v, wq_v, wk_v, wv_v, wg_v, wo_v, wu_v, wd_v,
     send1, recv1, ret, mix, send2, recv2, sums2, rsums2, hid, down, out_v,
     load_sem, s1_sem, r1_sem, sr_sem, rr_sem, sm_sem, rm_sem, s2_sem, r2_sem, ss_sem, rs_sem, sh_sem, rh_sem,
-    sd_sem, rd_sem, store_sem,
+    sd_sem, rd_sem,
 ):
     me_kv = lax.axis_index("kv")
     me_tp = lax.axis_index("tp")
@@ -60,6 +60,7 @@
     l_g1 = load(norm_gain, gain1_v)
     l_w = [load(a, b) for a, b in ((w_query, wq_v), (w_key, wk_v), (w_value, wv_v), (w_gate, wg_v))]
     l_freq = load(freq, freq_v)
+    l_pos = load(positions, pos_s)
     l_state = load(state, st_v)
     l_wo = load(w_out, wo_v)
     l_g2 = load(mlp_gain, gain2_v)
@@ -86,45 +87,58 @@
     normed = (inputs * gain1_v[...]).astype(BF16)
     extra = split_high_low(jnp.sum(inputs * inputs, axis=1, keepdims=True))
     for j in range(kv):
-        send1[j, :, 4 * ret_width:] = extra[j * seqs:(j + 1) * seqs].astype(BF16)
+        send1[0, j, :, 2 * ret_width:] = extra[j * seqs:(j + 1) * seqs].astype(BF16)
 
     l_freq.wait()
+    l_pos.wait()
     row = lax.broadcasted_iota(jnp.int32, (seqs, head_size), 0)
     lane = lax.broadcasted_iota(jnp.int32, (seqs, head_size), 1)
     pos = jnp.zeros((seqs, head_size), F32)
     for b in range(seqs):
-        pos = jnp.where(row == b, positions[b].astype(F32), pos)
+        pos = jnp.where(row == b, pos_s[b].astype(F32), pos)
     angle = pos * freq_v[...]
     cosine = jnp.cos(angle)
     sine = jnp.where(lane < head_size // 2, -1.0, 1.0) * jnp.sin(angle)
 
     t1 = tile_of(ret_width)
+    copies = ([], [])
     for i, weight in enumerate((wq_v, wk_v, wv_v, wg_v)):
         l_w[i].wait()
         for n in range(ret_width // t1):
             term = jnp.dot(normed, weight[:, n * t1:(n + 1) * t1], preferred_element_type=F32)
-            at = i * ret_width + n * t1
+            at = (i % 2) * ret_width + n * t1
             for j in range(kv):
-                send1[j, :, at:at + t1] = term[j * seqs:(j + 1) * seqs].astype(BF16)
-
-    pl.semaphore_wait(barrier, kv + tp - 2)
-    pending = []
-    copies = []
-    for s in range(1, kv):
-        to = lax.rem(me_kv + s, kv)
-        copies.append(remote(send1.at[to], recv1.at[s - 1], s1_sem.at[s - 1], r1_sem.at[s - 1], "kv", to))
-    pending += copies
-    summed = send1[me_kv].astype(F32)
-    for s in range(1, kv):
-        copies[s - 1].wait_recv()
-        summed = summed + recv1[s - 1].astype(F32)
-    total = summed[:, 4 * ret_width:4 * ret_width + 1] + summed[:, 4 * ret_width + 128:4 * ret_width + 129]
+                send1[i // 2, j, :, at:at + t1] = term[j * seqs:(j + 1) * seqs].astype(BF16)
+        if i % 2 == 1:
+            if i == 1:
+                pl.semaphore_wait(barrier, kv + tp - 2)
+            p = i // 2
+            piece = pl.ds(0, 2 * ret_width + (256 if p == 0 else 0))
+            for s in range(1, kv):
+                to = lax.rem(me_kv + s, kv)
+                copies[p].append(
+                    remote(
+                        send1.at[p, to, :, piece], recv1.at[p, s - 1, :, piece],
+                        s1_sem.at[p, s - 1], r1_sem.at[p, s - 1], "kv", to,
+                    )
+                )
+    pending = copies[0] + copies[1]
+
+    def gathered(p, size):
+        result = send1[p, me_kv, :, :size].astype(F32)
+        for s in range(1, kv):
+            copies[p][s - 1].wait_recv()
+            result = result + recv1[p, s - 1, :, :size].astype(F32)
+        return result
+
+    summed = gathered(0, 2 * ret_width + 256)
+    total = summed[:, 2 * ret_width:2 * ret_width + 1] + summed[:, 2 * ret_width + 128:2 * ret_width + 129]
     scale1 = lax.rsqrt(total / D + 1e-06)
 
-    def stack(i):
+    def stack(values, i):
         base = i * ret_width
         return jnp.concatenate(
-            [summed[:, base + h * head_size:base + (h + 1) * head_size] * scale1 for h in range(heads)], axis=0
+            [values[:, base + h * head_size:base + (h + 1) * head_size] * scale1 for h in range(heads)], axis=0
         )
 
     cos_all = jnp.concatenate([cosine] * heads, axis=0)
@@ -134,24 +148,27 @@
         return x * cos_all + pltpu.roll(x, head_size // 2, 1) * sin_all
 
     count = seqs * heads
-    query = turn(stack(0))
-    key = turn(stack(1)) * head_size ** (-0.5)
-    value = stack(2)
-    gate = stack(3)
+    query = turn(stack(summed, 0))
+    key = turn(stack(summed, 1)) * head_size ** (-0.5)
     columns = jnp.transpose(
         jnp.concatenate([query, key, jnp.zeros((128 - 2 * count, head_size), F32)], axis=0)
     )
+    overlap = jnp.sum(query * key, axis=1, keepdims=True)
+    gammas = [
+        1.0 - jnp.exp2(jnp.full((1, head_size), -5.0, F32) - 5.0 * (me_tp * heads + h).astype(F32) / (HEADS - 1))
+        for h in range(heads)
+    ]
     l_state.wait()
-    reads = []
+    old_reads = []
     for h in range(heads):
-        index = (me_tp * heads + h).astype(F32)
-        gamma = 1.0 - jnp.exp2(jnp.full((1, head_size), -5.0, F32) - 5.0 * index / (HEADS - 1))
         for b in range(seqs):
             at = h * seqs + b
-            fresh = gamma * st_v[b, h] + columns[:, count + at:count + at + 1] * value[at:at + 1, :]
-            st_v[b, h] = fresh
-            reads.append(jnp.sum(columns[:, at:at + 1] * fresh, axis=0, keepdims=True))
-    read = jnp.concatenate(reads, axis=0)
+            old_reads.append(gammas[h] * jnp.sum(columns[:, at:at + 1] * st_v[b, h], axis=0, keepdims=True))
+    old_read = jnp.concatenate(old_reads, axis=0)
+    summed = gathered(1, 2 * ret_width)
+    value = stack(summed, 0)
+    gate = stack(summed, 1)
+    read = old_read + overlap * value
     read = read * lax.rsqrt(jnp.mean(read * read, axis=-1, keepdims=True) + 1e-06)
     kept = read * (gate / (1.0 + jnp.exp(-gate)))
     for h in range(heads):
@@ -161,35 +178,42 @@
         to = lax.rem(me_kv + s, kv)
         copies.append(remote(ret.at[me_kv], ret.at[me_kv], sr_sem.at[s - 1], rr_sem.at[s - 1], "kv", to))
     pending += copies
-    store_state = pltpu.make_async_copy(st_v, new_state, store_sem.at[0])
-    store_state.start()
+    for h in range(heads):
+        for b in range(seqs):
+            at = h * seqs + b
+            st_v[b, h] = gammas[h] * st_v[b, h] + columns[:, count + at:count + at + 1] * value[at:at + 1, :]
+
+    t2 = tile_of(width)
     l_wo.wait()
-    for s in range(1, kv):
-        copies[s - 1].wait_recv()
-    retained = jnp.concatenate([ret[j].astype(F32) for j in range(kv)], axis=0).astype(BF16)
-
-    def reduce_tp(terms_into, buffer, send_sem, recv_sem):
-        terms_into()
-        sent = []
+    mix_copies = []
+    for r in range(kv):
+        owner = lax.rem(me_kv + kv - r, kv)
+        if r > 0:
+            copies[r - 1].wait_recv()
+        block = ret[owner]
+        for n in range(width // t2):
+            cols = slice(n * t2, (n + 1) * t2)
+            mix[me_tp, owner, :, cols] = jnp.dot(block, wo_v[:, cols], preferred_element_type=F32).astype(BF16)
+        row_copies = []
         for s in range(1, tp):
             to = lax.rem(me_tp + s, tp)
-            sent.append(remote(buffer.at[me_tp], buffer.at[me_tp], send_sem.at[s - 1], recv_sem.at[s - 1], "tp", to))
-        for s in range(1, tp):
-            sent[s - 1].wait_recv()
-        result = buffer[0].astype(F32)
-        for j in range(1, tp):
-            result = result + buffer[j].astype(F32)
-        return result, sent
-
-    t2 = tile_of(width)
-
-    def out_terms():
-        for n in range(width // t2):
-            cols = slice(n * t2, (n + 1) * t2)
-            mix[me_tp, :, cols] = jnp.dot(retained, wo_v[:, cols], preferred_element_type=F32).astype(BF16)
-
-    head_sum, sent = reduce_tp(out_terms, mix, sm_sem, rm_sem)
-    pending += sent
+            row_copies.append(
+                remote(
+                    mix.at[me_tp, owner], mix.at[me_tp, owner], sm_sem.at[r, s - 1], rm_sem.at[r, s - 1], "tp", to
+                )
+            )
+        mix_copies.append(row_copies)
+        pending += row_copies
+    for row_copies in mix_copies:
+        for copy in row_copies:
+            copy.wait_recv()
+
+    def added(j):
+        return jnp.concatenate([mix[j, k].astype(F32) for k in range(kv)], axis=0)
+
+    head_sum = added(0)
+    for j in range(1, tp):
+        head_sum = head_sum + added(j)
     mixed = (inputs + head_sum).astype(BF16)
     middle = mixed.astype(F32)
     l_g2.wait()
@@ -247,30 +271,50 @@
         hid_copies.append(row_copies)
         pending += row_copies
 
+    last = []
     for c in range(chunks):
         l_down[c].wait()
         for s in range(1, kv):
             hid_copies[c][s - 1].wait_recv()
         hidden = jnp.concatenate([hid[c, j].astype(F32) for j in range(kv)], axis=0).astype(BF16)
-
-        @pl.loop(0, width // t2)
-        def _(n, c=c, hidden=hidden):
-            cols = pl.ds(pl.multiple_of(n * t2, t2), t2)
-            term = jnp.dot(hidden, wd_v[pl.ds(c * cw, cw), cols], preferred_element_type=F32)
-            if c == 0:
+        for n in range(width // t2):
+            cols = slice(n * t2, (n + 1) * t2)
+            term = jnp.dot(hidden, wd_v[c * cw:(c + 1) * cw, cols], preferred_element_type=F32)
+            if c > 0:
+                term = term + out_v[:, cols]
+            if c < chunks - 1:
                 out_v[:, cols] = term
-            else:
-                out_v[:, cols] += term
-
-    def down_terms():
-        down[me_tp] = out_v[...].astype(BF16)
-
-    down_sum, sent = reduce_tp(down_terms, down, sd_sem, rd_sem)
-    pending += sent
-    out_ref[...] = (middle + down_sum).astype(BF16)
+                continue
+            down[me_tp, n] = term.astype(BF16)
+            row_copies = []
+            for s in range(1, tp):
+                to = lax.rem(me_tp + s, tp)
+                row_copies.append(
+                    remote(
+                        down.at[me_tp, n], down.at[me_tp, n], sd_sem.at[n, s - 1], rd_sem.at[n, s - 1], "tp", to
+                    )
+                )
+            last.append(row_copies)
+            pending += row_copies
+    for n in range(width // t2):
+        for copy in last[n]:
+            copy.wait_recv()
+        total = down[0, n].astype(F32)
+        for j in range(1, tp):
+            total = total + down[j, n].astype(F32)
+        cols = slice(n * t2, (n + 1) * t2)
+        out_ref[:, cols] = (middle[:, cols] + total).astype(BF16)
     for copy in pending:
         copy.wait_send()
-    store_state.wait()
+
+
+def finish(made, fresh, out_ref, new_state, sem):
+    first = pltpu.make_async_copy(fresh, new_state, sem.at[0])
+    second = pltpu.make_async_copy(made, out_ref, sem.at[1])
+    first.start()
+    second.start()
+    first.wait()
+    second.wait()
 
 
 def solution(mesh):
@@ -288,20 +332,22 @@
         half = head_size // 2
         table = 10000.0 ** (-(np.arange(half) * 2.0) / head_size)
         freq = jnp.asarray(np.concatenate([table, table])[None, :], F32)
-        any_spec = pl.BlockSpec(memory_space=pl.ANY)
+        any_spec = pl.BlockSpec(memory_space=pltpu.HBM)
         vmem = pltpu.VMEM
         dma = pltpu.SemaphoreType.DMA
-        block1 = 4 * ret_width + 256
-        return pl.pallas_call(
+        block1 = 2 * ret_width + 256
+        parts = width // tile_of(width)
+        made, fresh = pl.pallas_call(
             functools.partial(kernel, kv, tp, chunks),
             name="layer",
             out_shape=(
-                jax.ShapeDtypeStruct((rows, width), BF16),
-                jax.ShapeDtypeStruct(state.shape, F32),
+                pltpu.VMEM((rows, width), BF16),
+                pltpu.VMEM(state.shape, F32),
             ),
-            in_specs=[pl.BlockSpec(memory_space=pltpu.SMEM)] + [any_spec] * 12,
-            out_specs=(pl.BlockSpec(memory_space=pltpu.VMEM), any_spec),
+            in_specs=[any_spec] * 13,
+            out_specs=(pl.BlockSpec(memory_space=pltpu.VMEM), pl.BlockSpec(memory_space=pltpu.VMEM)),
             scratch_shapes=[
+                pltpu.SMEM(positions.shape, jnp.int32),
                 vmem((rows, width), BF16),
                 vmem((1, width), F32),
                 vmem((1, width), F32),
@@ -313,35 +359,50 @@
                 vmem(w_out.shape, BF16),
                 vmem(w_up.shape, BF16),
                 vmem(w_down.shape, BF16),
-                vmem(state.shape, F32),
-                vmem((kv, seqs, block1), BF16),
-                vmem((kv - 1, seqs, block1), BF16),
+                vmem((2, kv, seqs, block1), BF16),
+                vmem((2, kv - 1, seqs, block1), BF16),
                 vmem((kv, seqs, ret_width), BF16),
-                vmem((tp, rows, width), BF16),
+                vmem((tp, kv, seqs, width), BF16),
                 vmem((chunks, kv, seqs, cw), BF16),
                 vmem((chunks, kv - 1, seqs, cw), BF16),
                 vmem((kv, seqs, 256), BF16),
                 vmem((kv - 1, seqs, 256), BF16),
                 vmem((chunks, kv, seqs, cw), BF16),
-                vmem((tp, rows, width), BF16),
+                vmem((tp, parts, rows, width // parts), BF16),
                 vmem((rows, width), F32),
-                dma((10 + 2 * chunks,)),
+                dma((11 + 2 * chunks,)),
+                dma((2, kv - 1)), dma((2, kv - 1)),
                 dma((kv - 1,)), dma((kv - 1,)),
-                dma((kv - 1,)), dma((kv - 1,)),
-                dma((tp - 1,)), dma((tp - 1,)),
+                dma((kv, tp - 1)), dma((kv, tp - 1)),
                 dma((chunks, kv - 1)), dma((chunks, kv - 1)),
                 dma((kv - 1,)), dma((kv - 1,)),
                 dma((chunks, kv - 1)), dma((chunks, kv - 1)),
-                dma((tp - 1,)), dma((tp - 1,)),
-                dma((1,)),
+                dma((parts, tp - 1)), dma((parts, tp - 1)),
             ],
             compiler_params=pltpu.CompilerParams(
-                collective_id=0, has_side_effects=True, vmem_limit_bytes=60 * 1024 * 1024
+                collective_id=0, has_side_effects=True, vmem_limit_bytes=48 * 1024 * 1024
             ),
         )(
-            positions, tokens, state, norm_gain[None, :], freq, w_query, w_key, w_value, w_gate, w_out,
-            mlp_gain[None, :], w_up, w_down,
+            *[
+                pltpu.with_memory_space_constraint(x, pltpu.HBM)
+                for x in (
+                    positions, tokens, state, norm_gain[None, :], freq, w_query, w_key, w_value, w_gate, w_out,
+                    mlp_gain[None, :], w_up, w_down,
+                )
+            ],
         )
+        return pl.pallas_call(
+            finish,
+            name="finish",
+            out_shape=(
+                jax.ShapeDtypeStruct((rows, width), BF16),
+                jax.ShapeDtypeStruct(state.shape, F32),
+            ),
+            in_specs=[pl.BlockSpec(memory_space=pltpu.VMEM)] * 2,
+            out_specs=(any_spec, any_spec),
+            scratch_shapes=[pltpu.SemaphoreType.DMA((2,))],
+            compiler_params=pltpu.CompilerParams(vmem_limit_bytes=4 * 1024 * 1024),
+        )(made, fresh)
 
     return jax.shard_map(
         shards,

time: 36.9 us -> 32.4 us (0.88)
  local copies, waits for them, and re-layouts: 3.67 us -> 0 us
  Pallas kernels: 32.4 us -> 31.6 us
    unnamed x2 -> x0, local copies, waits for them, and re-layouts: 3.67 us -> none
    pallas_call x1, Pallas kernels: 32.4 us -> 30.6 us  [shards(): pl.pallas_call(functools.partial(kernel, kv, tp, chunks), name='layer', o...]
    pallas_call x0 -> x1, Pallas kernels: none -> 0.99 us  [shards(): pl.pallas_call(finish, name='finish', out_shape=(jax.ShapeDtypeStruct((ro...]
where the time goes in v2:
time: 32.4 us; the launch traced here: 32.3 us
  Pallas kernels  31.6 us (98%)
  between operations  0.64 us (2%)
    pallas_call x1, Pallas kernels, shards(): pl.pallas_call(functools.partial(kernel, kv, tp, chunks), name='layer', o...  30.6 us
    pallas_call x1, Pallas kernels, shards(): pl.pallas_call(finish, name='finish', out_shape=(jax.ShapeDtypeStruct((ro...  0.99 us

profile of v2, /device:TPU:0, one launch (start us, length us, event | category | flops | bytes accessed | tf_op | source)
XLA Modules:
  0.0 32.3 jit_solution(11421840655976435274)
XLA Ops:
  0.6 30.6 %layer.1 = (bf16[16,1024]{1,0:T(8,128)(2,1)S(1)}, f32[4,4,128,128]{3,2,1,0:T(8,128)S(1)}) custom-call(s32[4]{0:T(128)} %positions.1, bf16[16,1024]{1,0:T(8,128)(2,1)} %tokens.1, f32[4,4,128,128]{3,2,1,0:T(8,128)} %state.1, f32[1,1024]{1,0:T(1,128)} %bitcast.2, f32[1,128]{1,0:T(1,128)} %constant.2.clone.freq, bf16[1024,512]{1,0:T(8,128)(2,1)} %w_query.1, ...), custom_call_target="tpu_custom_call" | custom-call | tf_op jit(solution)/shard_map/layer/pallas_call | solution.py:340
  31.3 1.0 %finish.1 = (bf16[16,1024]{1,0:T(8,128)(2,1)}, f32[4,4,128,128]{3,2,1,0:T(8,128)}) custom-call(bf16[16,1024]{1,0:T(8,128)(2,1)S(1)} %get-tuple-element.4.made, f32[4,4,128,128]{3,2,1,0:T(8,128)S(1)} %get-tuple-element.5.fresh), custom_call_target="tpu_custom_call" | custom-call | tf_op jit(solution)/shard_map/finish/pallas_call | solution.py:394

commit v3 on v2

--- a/solution.py
+++ b/solution.py
@@ -69,9 +69,14 @@
 
     barrier = pltpu.get_barrier_semaphore()
     for s in range(1, kv):
-        pl.semaphore_signal(barrier, inc=1, device_id={"kv": lax.rem(me_kv + s, kv)}, device_id_type=MESH)
+        pl.semaphore_signal(barrier, inc=1, device_id={"kv": (me_kv + s) % kv}, device_id_type=MESH)
     for s in range(1, tp):
         pl.semaphore_signal(barrier, inc=1, device_id={"tp": lax.rem(me_tp + s, tp)}, device_id_type=MESH)
+
+    upper = (2 * me_kv) // kv
+
+    def offset(s):
+        return upper * s + (1 - upper) * (kv - s)
 
     def remote(src, dst, send_sem, recv_sem, axis, target):
         copy = pltpu.make_async_remote_copy(
@@ -115,11 +120,11 @@
             p = i // 2
             piece = pl.ds(0, 2 * ret_width + (256 if p == 0 else 0))
             for s in range(1, kv):
-                to = lax.rem(me_kv + s, kv)
+                to = lax.rem(me_kv + offset(s), kv)
                 copies[p].append(
                     remote(
-                        send1.at[p, to, :, piece], recv1.at[p, s - 1, :, piece],
-                        s1_sem.at[p, s - 1], r1_sem.at[p, s - 1], "kv", to,
+                        send1.at[p, to, :, piece], recv1.at[p, offset(s) - 1, :, piece],
+                        s1_sem.at[p, s - 1], r1_sem.at[p, offset(s) - 1], "kv", to,
                     )
                 )
     pending = copies[0] + copies[1]
@@ -128,7 +133,7 @@
         result = send1[p, me_kv, :, :size].astype(F32)
         for s in range(1, kv):
             copies[p][s - 1].wait_recv()
-            result = result + recv1[p, s - 1, :, :size].astype(F32)
+            result = result + recv1[p, offset(s) - 1, :, :size].astype(F32)
         return result
 
     summed = gathered(0, 2 * ret_width + 256)
@@ -175,8 +180,8 @@
         ret[me_kv, :, h * head_size:(h + 1) * head_size] = kept[h * seqs:(h + 1) * seqs].astype(BF16)
     copies = []
     for s in range(1, kv):
-        to = lax.rem(me_kv + s, kv)
-        copies.append(remote(ret.at[me_kv], ret.at[me_kv], sr_sem.at[s - 1], rr_sem.at[s - 1], "kv", to))
+        to = lax.rem(me_kv + offset(s), kv)
+        copies.append(remote(ret.at[me_kv], ret.at[me_kv], sr_sem.at[s - 1], rr_sem.at[offset(s) - 1], "kv", to))
     pending += copies
     for h in range(heads):
         for b in range(seqs):
@@ -187,7 +192,7 @@
     l_wo.wait()
     mix_copies = []
     for r in range(kv):
-        owner = lax.rem(me_kv + kv - r, kv)
+        owner = me_kv if r == 0 else lax.rem(me_kv + kv - offset(r), kv)
         if r > 0:
             copies[r - 1].wait_recv()
         block = ret[owner]
@@ -223,8 +228,8 @@
         sums2[j] = extra[j * seqs:(j + 1) * seqs].astype(BF16)
     sum_copies = []
     for s in range(1, kv):
-        to = lax.rem(me_kv + s, kv)
-        sum_copies.append(remote(sums2.at[to], rsums2.at[s - 1], ss_sem.at[s - 1], rs_sem.at[s - 1], "kv", to))
+        to = lax.rem(me_kv + offset(s), kv)
+        sum_copies.append(remote(sums2.at[to], rsums2.at[offset(s) - 1], ss_sem.at[s - 1], rs_sem.at[offset(s) - 1], "kv", to))
     pending += sum_copies
 
     t3 = tile_of(cw)
@@ -241,9 +246,9 @@
 
         row_copies = []
         for s in range(1, kv):
-            to = lax.rem(me_kv + s, kv)
+            to = lax.rem(me_kv + offset(s), kv)
             row_copies.append(
-                remote(send2.at[c, to], recv2.at[c, s - 1], s2_sem.at[c, s - 1], r2_sem.at[c, s - 1], "kv", to)
+                remote(send2.at[c, to], recv2.at[c, offset(s) - 1], s2_sem.at[c, s - 1], r2_sem.at[c, offset(s) - 1], "kv", to)
             )
         up_copies.append(row_copies)
         pending += row_copies
@@ -251,7 +256,7 @@
     sums = sums2[me_kv].astype(F32)
     for s in range(1, kv):
         sum_copies[s - 1].wait_recv()
-        sums = sums + rsums2[s - 1].astype(F32)
+        sums = sums + rsums2[offset(s) - 1].astype(F32)
     scale2 = lax.rsqrt((sums[:, :1] + sums[:, 128:129]) / D + 1e-06)
 
     hid_copies = []
@@ -259,14 +264,14 @@
         up_sum = send2[c, me_kv].astype(F32)
         for s in range(1, kv):
             up_copies[c][s - 1].wait_recv()
-            up_sum = up_sum + recv2[c, s - 1].astype(F32)
+            up_sum = up_sum + recv2[c, offset(s) - 1].astype(F32)
         positive = jnp.maximum(up_sum * scale2, 0.0)
         hid[c, me_kv] = (positive * positive).astype(BF16)
         row_copies = []
         for s in range(1, kv):
-            to = lax.rem(me_kv + s, kv)
+            to = lax.rem(me_kv + offset(s), kv)
             row_copies.append(
-                remote(hid.at[c, me_kv], hid.at[c, me_kv], sh_sem.at[c, s - 1], rh_sem.at[c, s - 1], "kv", to)
+                remote(hid.at[c, me_kv], hid.at[c, me_kv], sh_sem.at[c, s - 1], rh_sem.at[c, offset(s) - 1], "kv", to)
             )
         hid_copies.append(row_copies)
         pending += row_copies

time: 32.4 us -> 31.8 us (0.981)
  Pallas kernels: 31.6 us -> 31 us
    pallas_call x1, Pallas kernels: 30.6 us -> 30 us  [shards(): pl.pallas_call(functools.partial(kernel, kv, tp, chunks), name='layer', o...]
where the time goes in v3:
time: 31.8 us; the launch traced here: 31.6 us
  Pallas kernels  31 us (97%)
  between operations  0.64 us (2%)
    pallas_call x1, Pallas kernels, shards(): pl.pallas_call(functools.partial(kernel, kv, tp, chunks), name='layer', o...  30 us
    pallas_call x1, Pallas kernels, shards(): pl.pallas_call(finish, name='finish', out_shape=(jax.ShapeDtypeStruct((ro...  0.99 us

profile of v3, /device:TPU:0, one launch (start us, length us, event | category | flops | bytes accessed | tf_op | source)
XLA Modules:
  0.0 31.6 jit_solution(1411042979177113290)
XLA Ops:
  0.6 30.0 %layer.1 = (bf16[16,1024]{1,0:T(8,128)(2,1)S(1)}, f32[4,4,128,128]{3,2,1,0:T(8,128)S(1)}) custom-call(s32[4]{0:T(128)} %positions.1, bf16[16,1024]{1,0:T(8,128)(2,1)} %tokens.1, f32[4,4,128,128]{3,2,1,0:T(8,128)} %state.1, f32[1,1024]{1,0:T(1,128)} %bitcast.2, f32[1,128]{1,0:T(1,128)} %constant.2.clone.freq, bf16[1024,512]{1,0:T(8,128)(2,1)} %w_query.1, ...), custom_call_target="tpu_custom_call" | custom-call | tf_op jit(solution)/shard_map/layer/pallas_call | solution.py:345
  30.6 1.0 %finish.1 = (bf16[16,1024]{1,0:T(8,128)(2,1)}, f32[4,4,128,128]{3,2,1,0:T(8,128)}) custom-call(bf16[16,1024]{1,0:T(8,128)(2,1)S(1)} %get-tuple-element.4.made, f32[4,4,128,128]{3,2,1,0:T(8,128)S(1)} %get-tuple-element.5.fresh), custom_call_target="tpu_custom_call" | custom-call | tf_op jit(solution)/shard_map/finish/pallas_call | solution.py:399
